TPU v7x, 128 devices: a whole 4x4x4 slice. The times are simulated.
128 devices in a mesh: fs: 16 (over z, y), tp: 8 (over x, core).
Axes of the slice: x: 4, y: 4, z: 4, core: 2. Of those that a mesh axis runs over, the one named last changes fastest.
Arguments:
- late_input: bfloat16 [8192, 2048], P(('fs', 'tp')), may hold values from -6 to 6
- early_input: bfloat16 [8192, 2048], P(('fs', 'tp')), may hold values from -6 to 6
- early_grad: bfloat16 [8192, 2048], P(('fs', 'tp')), may hold values from -24 to 24
- pre_gain: float32 [2048], replicated, may hold values from 0.1 to 1.9
- post_gain: float32 [2048], replicated, may hold values from 0.1 to 1.9
- gate_weight: bfloat16 [2048, 4096], P('fs', 'tp'), may hold values from -0.125 to 0.125
- up_weight: bfloat16 [2048, 4096], P('fs', 'tp'), may hold values from -0.125 to 0.125
- down_weight: bfloat16 [2048, 4096], P('fs', 'tp'), may hold values from -0.09375 to 0.09375
- gate_sum: float32 [2048, 4096], P('fs', 'tp'), may hold values from -1.8 to 1.8
- up_sum: float32 [2048, 4096], P('fs', 'tp'), may hold values from -1.8 to 1.8
- down_gradient_sum: float32 [2048, 4096], P('fs', 'tp'), may hold values from -1.8 to 1.8
Outputs:
- late_output: bfloat16 [8192, 2048], P(('fs', 'tp'))
- early_input_grad: bfloat16 [8192, 2048], P(('fs', 'tp'))
- gate_total: float32 [2048, 4096], P('fs', 'tp')
- up_total: float32 [2048, 4096], P('fs', 'tp')
- down_total: float32 [2048, 4096], P('fs', 'tp')
All inputs are finite; a program needn't handle non-finite values.
Results may differ from a plain program's by a relative error of at most 0.013.
Values may be sent and summed in bfloat16 or wider, within the bound.
A program may use at most 128 MiB of HBM per device.

v0:
```python
import math
import jax
import jax.numpy as jnp
from jax import lax
from jax.sharding import PartitionSpec as P

NORM_EPS = 1e-06


def sent_together(arrays, axis, dim, along):
    ends, at = ([], 0)
    for a in arrays[:-1]:
        at += a.shape[along]
        ends.append(at)
    both = jnp.concatenate(arrays, axis=along)
    return tuple(jnp.split(lax.all_gather(both, axis, axis=dim, tiled=True), ends, axis=along))


def sent_to_all(shard, axis):
    peers = lax.axis_size(axis)
    return lax.all_to_all(
        jnp.broadcast_to(shard[None], (peers, *shard.shape)), axis, 0, 0, tiled=True
    )


def in_order(parts, dim):
    parts = jnp.moveaxis(parts, 0, dim)
    dims = parts.shape
    return parts.reshape(*dims[:dim], dims[dim] * dims[dim + 1], *dims[dim + 2 :])


def gather_directly(shard, axis, dim):
    parts = sent_to_all(shard, axis)
    return in_order(parts, dim)


def in_blocks(shard, dim, peers):
    dims = shard.shape
    parts = shard.reshape(*dims[:dim], peers, dims[dim] // peers, *dims[dim + 1 :])
    return jnp.moveaxis(parts, dim, 0)


def summed_on_arrival(shard, axis, dim):
    parts = in_blocks(shard, dim, lax.axis_size(axis))
    arrived = lax.all_to_all(parts, axis, split_axis=0, concat_axis=0, tiled=True)
    return arrived.astype(jnp.float32).sum(axis=0)


def contract_last(first_op, second_op):
    return lax.dot_general(
        first_op, second_op, (((1,), (1,)), ((), ())), preferred_element_type=jnp.float32
    )


def contract_first(first_op, second_op):
    return lax.dot_general(
        first_op, second_op, (((0,), (0,)), ((), ())), preferred_element_type=jnp.float32
    )


def inverse_rms(values):
    return lax.rsqrt(jnp.mean(values * values, axis=-1, keepdims=True) + NORM_EPS)


def per_device(
    late_input,
    early_input,
    early_grad,
    pre_gain,
    post_gain,
    gate_weight,
    up_weight,
    down_weight,
    gate_sum,
    up_sum,
    down_gradient_sum,
):
    tok_rows, model_width = late_input.shape
    group_rows = tok_rows * lax.axis_size("tp")
    grad_scale = 1.0 / math.sqrt(group_rows * lax.axis_size("fs"))
    hidden_width = gate_sum.shape[1]
    input_rows = jnp.stack([late_input, early_input]).astype(jnp.float32)
    input_inverse = inverse_rms(input_rows)
    normed = (input_rows * input_inverse * pre_gain).astype(jnp.bfloat16)
    normed_rows = lax.all_gather(normed, "tp", axis=1, tiled=True)
    gate_all, up_all, down_gradient_rows = sent_together(
        (gate_weight, up_weight, down_weight), "fs", 0, 1
    )
    flat_rows = normed_rows.reshape(2 * group_rows, model_width)
    gate_pre = jnp.dot(flat_rows, gate_all, preferred_element_type=jnp.float32)
    up_pre = jnp.dot(flat_rows, up_all, preferred_element_type=jnp.float32)
    hidden_state = (
        (jax.nn.silu(gate_pre) * up_pre).astype(jnp.bfloat16).reshape(2, group_rows, hidden_width)
    )
    gated_product = jnp.einsum(
        "utx,ix->tui", hidden_state, down_gradient_rows, preferred_element_type=jnp.float32
    )
    mixed_sum = lax.psum_scatter(
        gated_product.reshape(lax.axis_size("tp") * tok_rows, 2 * model_width).astype(jnp.bfloat16),
        "tp",
        scatter_dimension=0,
        tiled=True,
    ).astype(jnp.float32)
    mixed_sum = lax.optimization_barrier(mixed_sum.astype(jnp.bfloat16)).astype(jnp.float32)
    mixed_sum = mixed_sum.reshape(tok_rows, 2, model_width)
    mixed_inverse = inverse_rms(mixed_sum)
    late_output = (input_rows[0] + 0.5 * mixed_sum[:, 0] * mixed_inverse[:, 0] * post_gain).astype(
        jnp.bfloat16
    )
    early_mixed = mixed_sum[:, 1]
    early_inverse_norm = mixed_inverse[:, 1]
    weighted = 0.5 * early_grad.astype(jnp.float32) * post_gain
    mixed_cot = (
        early_inverse_norm * weighted
        - early_mixed
        * early_inverse_norm**3
        * jnp.mean(weighted * early_mixed, axis=-1, keepdims=True)
    ).astype(jnp.bfloat16)
    cot_rows = gather_directly(mixed_cot, "tp", 0)
    early_hidden = hidden_state[1]
    early_normed = normed_rows[1]
    hidden_cot = jnp.dot(cot_rows, down_gradient_rows, preferred_element_type=jnp.float32)
    early_gate = gate_pre[group_rows:]
    early_up = up_pre[group_rows:]
    sigmoid_gate = jax.nn.sigmoid(early_gate)
    gate_cot = (
        hidden_cot * early_up * sigmoid_gate * (1.0 + early_gate * (1.0 - sigmoid_gate))
    ).astype(jnp.bfloat16)
    up_cot = (hidden_cot * early_gate * sigmoid_gate).astype(jnp.bfloat16)
    normed_cot = summed_on_arrival(
        (contract_last(gate_cot, gate_all) + contract_last(up_cot, up_all)).astype(jnp.bfloat16),
        "tp",
        0,
    )
    normed_cot = lax.optimization_barrier(normed_cot.astype(jnp.bfloat16)).astype(jnp.float32)
    weighted_in = normed_cot * pre_gain
    early_values = input_rows[1]
    early_in_inverse = input_inverse[1]
    early_input_grad = (
        early_grad.astype(jnp.float32)
        + early_in_inverse * weighted_in
        - early_values
        * early_in_inverse**3
        * jnp.mean(weighted_in * early_values, axis=-1, keepdims=True)
    ).astype(jnp.bfloat16)
    totals = lax.psum_scatter(
        (
            grad_scale
            * jnp.concatenate(
                [
                    contract_first(early_normed, gate_cot),
                    contract_first(early_normed, up_cot),
                    contract_first(cot_rows, early_hidden),
                ],
                1,
            )
        ).astype(jnp.bfloat16),
        "fs",
        scatter_dimension=0,
        tiled=True,
    ).astype(jnp.float32)
    gate_total = gate_sum + totals[:, :hidden_width]
    up_total = up_sum + totals[:, hidden_width : 2 * hidden_width]
    down_total = down_gradient_sum + totals[:, 2 * hidden_width :]
    return (late_output, early_input_grad, gate_total, up_total, down_total)


def solution(mesh):
    in_specs = (
        P(("fs", "tp"), None),
        P(("fs", "tp"), None),
        P(("fs", "tp"), None),
        P(),
        P(),
        P("fs", "tp"),
        P("fs", "tp"),
        P("fs", "tp"),
        P("fs", "tp"),
        P("fs", "tp"),
        P("fs", "tp"),
    )
    out_specs = (
        P(("fs", "tp"), None),
        P(("fs", "tp"), None),
        P("fs", "tp"),
        P("fs", "tp"),
        P("fs", "tp"),
    )
    return jax.shard_map(
        per_device, mesh=mesh, in_specs=in_specs, out_specs=out_specs, check_vma=False
    )
```

profile of v0, /device:TPU:0, one launch (start us, length us, event | category | flops | bytes accessed | tf_op | source)
XLA Modules:
  0.0 314.3 jit_solution(15130578604359886631)
XLA Ops:
  7.2 1.2 multiply_reduce_fusion.1
  8.4 2.0 multiply_convert_fusion.2
  10.5 1.8 pad_maximum_fusion
  12.4 32.7 %all-gather.5.cloned.1.call-done = bf16[2,512,2048]{2,1,0:T(8,128)(2,1)} async-done(((bf16[2,64,2048]{2,1,0:T(8,128)(2,1)}), bf16[2,512,2048]{2,1,0:T(8,128)(2,1)}) %all-gather.5.cloned.1.call-update) | async-done | bytes 4194320 | tf_op jit(solution)/shard_map/all_gather | solution.py:85
  45.2 63.5 %all-gather.3.cloned.1.call-done = bf16[2048,1536]{1,0:T(8,128)(2,1)} async-done(((bf16[128,1536]{1,0:T(8,128)(2,1)}), bf16[2048,1536]{1,0:T(8,128)(2,1)}) %all-gather.3.cloned.1.call-update) | async-done | bytes 6291472 | tf_op jit(solution)/shard_map/all_gather | solution.py:16
  108.7 5.3 %fusion.9 = f32[1024,512]{1,0:T(8,128)S(1)} fusion(bf16[1024,2048]{1,0:T(8,128)(2,1)} %bitcast.66, bf16[2048,1536]{1,0:T(8,128)(2,1)} %all-gather.3.cloned.1.call-done), kind=kOutput, calls=%fused_computation.14 | convolution fusion | flops 2147483648 | bytes 8388608 | tf_op jit(solution)/shard_map/dot_general | solution.py:90
  114.6 3.9 %multiply_convert_fusion = (bf16[1024,512]{1,0:T(8,128)(2,1)S(1)}, f32[1024,512]{1,0:T(8,128)}) fusion(f32[1024,512]{1,0:T(8,128)S(1)} %fusion.9, bf16[1024,2048]{1,0:T(8,128)(2,1)S(1)} %bitcast.67, bf16[2048,1536]{1,0:T(8,128)(2,1)S(1)} %copy-done.2), kind=kOutput, calls=%fused_computation.6 | convolution fusion | flops 2150629376 | bytes 11534336 | tf_op jit(solution)/shard_map/dot_general | solution.py:91
  118.5 4.4 %convolution_convert_fusion = bf16[2048,2,512]{2,0,1:T(8,128)(2,1)} fusion(bf16[2,512,512]{2,1,0:T(8,128)(2,1)S(1)} %bitcast.75, bf16[2048,1536]{1,0:T(8,128)(2,1)S(1)} %copy-done.2), kind=kOutput, calls=%fused_computation.3 | convolution fusion | flops 2149580800 | bytes 7340032 | tf_op jit(solution)/shard_map/utx,ix->tui/dot_general | solution.py:95
  122.9 6.3 %copy.39 = bf16[512,4096]{1,0:T(8,128)(2,1)} copy(bf16[512,4096]{0,1:T(8,128)(2,1)} %bitcast.68) | data formatting | bytes 8388608 | tf_op jit(solution)/shard_map/convert_element_type | solution.py:99
  129.9 36.9 %reduce-scatter.5.cloned.1.call-done = bf16[64,4096]{1,0:T(8,128)(2,1)} async-done(((bf16[512,4096]{1,0:T(8,128)(2,1)}), bf16[64,4096]{1,0:T(8,128)(2,1)}) %reduce-scatter.5.cloned.1.call-update) | async-done | bytes 524304 | tf_op jit(solution)/shard_map/reduce_scatter | solution.py:98
  166.9 2.1 reshape.128
  168.9 1.6 fusion.31
  172.0 29.7 %all_to_all.10 = bf16[8,64,2048]{2,1,0:T(8,128)(2,1)S(1)} all-to-all(bf16[8,64,2048]{2,1,0:T(8,128)(2,1)S(1)} %broadcast_in_dim.2), channel_id=1, replica_groups=mesh['fs'=16,'tp'=8] {'tp'}, dimensions={0} | all-to-all | bytes 4194304 | tf_op jit(solution)/shard_map/all_to_all | solution.py:21
  201.6 1.3 fusion.24
  203.8 3.3 %multiply_convert_fusion.1 = (bf16[512,512]{1,0:T(8,128)(2,1)S(1)}, bf16[512,512]{1,0:T(8,128)(2,1)S(1)}) fusion(f32[1024,512]{1,0:T(8,128)S(1)} %copy-done.13, f32[1024,512]{1,0:T(8,128)S(1)} %copy-done.14, bf16[512,2048]{1,0:T(8,128)(2,1)S(1)} %bitcast.65, bf16[2048,1536]{1,0:T(8,128)(2,1)} %all-gather.3.cloned.1.call-done), kind=kOutput, calls=%fused_computation.23 | convolution fusion | flops 1077149696 | bytes 7340032 | tf_op jit(solution)/shard_map/dot_general | solution.py:122
  207.1 1.3 fusion.2
  208.4 1.3 fusion.3
  209.8 3.8 %fusion = bf16[2048,1536]{0,1:T(8,128)(2,1)} fusion(f32[2048,512]{0,1:T(8,128)S(1)} %fusion.24, f32[2048,512]{0,1:T(8,128)S(1)} %fusion.2, f32[2048,512]{0,1:T(8,128)S(1)} %fusion.3), kind=kLoop, calls=%fused_computation.1 | loop fusion | flops 12582912 | bytes 18874368 | tf_op jit(solution)/shard_map/convert_element_type | solution.py:157
  213.6 8.6 %copy.48 = bf16[2048,1536]{1,0:T(8,128)(2,1)} copy(bf16[2048,1536]{0,1:T(8,128)(2,1)} %fusion) | data formatting | bytes 12582912
  222.3 2.9 fusion.7
  225.1 4.2 %add_convert_fusion = bf16[512,2048]{1,0:T(8,128)(2,1)} fusion(f32[512,2048]{1,0:T(8,128)S(1)} %fusion.7, bf16[512,512]{1,0:T(8,128)(2,1)S(1)} %get-tuple-element.25, bf16[2048,1536]{1,0:T(8,128)(2,1)} %all-gather.3.cloned.1.call-done), kind=kOutput, calls=%fused_computation.2 | convolution fusion | flops 1075838976 | bytes 8912896 | tf_op jit(solution)/shard_map/dot_general | solution.py:50
  229.4 3.8 %all-to-all-start.1 = ((bf16[8,64,2048]{2,1,0:T(8,128)(2,1)}), bf16[8,64,2048]{2,1,0:T(8,128)(2,1)S(1)}, u32[]{:S(2)}, u32[]{:S(2)}) async-start(bf16[8,64,2048]{2,1,0:T(8,128)(2,1)} %bitcast.14), calls=%async_computation.2 | async-start | bytes 4194304 | tf_op jit(solution)/shard_map/all_to_all | solution.py:45
  233.1 0.8 copy.44
  234.0 0.8 copy.43
  235.7 1.1 maximum_convert_fusion
  236.8 23.5 %all-to-all-done.1 = bf16[8,64,2048]{2,1,0:T(8,128)(2,1)S(1)} async-done(((bf16[8,64,2048]{2,1,0:T(8,128)(2,1)}), bf16[8,64,2048]{2,1,0:T(8,128)(2,1)S(1)}, u32[]{:S(2)}, u32[]{:S(2)}) %all-to-all-start.1) | async-done | bytes 2097184 | tf_op jit(solution)/shard_map/all_to_all | solution.py:45
  260.2 1.1 reduce_sum.51
  261.3 1.2 multiply_reduce_fusion.2
  262.6 2.2 fusion.23
  264.8 39.1 %reduce-scatter.7.cloned.1.call-done = bf16[128,1536]{1,0:T(8,128)(2,1)} async-done(((bf16[2048,1536]{1,0:T(8,128)(2,1)}), bf16[128,1536]{1,0:T(8,128)(2,1)}) %reduce-scatter.7.cloned.1.call-update) | async-done | bytes 393232
  303.8 1.2 copy.49
  305.2 0.8 copy.45
  (56 shorter events, 6.4 us)
Async XLA Ops:
  7.2 38.0 %all-gather.5.cloned.1.call-start = ((), (), s32[]{:S(2)}) async-start(), calls=%async_computation.5 | async-start | bytes 4718592 | tf_op jit(solution)/shard_map/all_gather | solution.py:85
  10.5 98.2 %all-gather.3.cloned.1.call-start = ((), (), s32[]{:S(2)}) async-start(), calls=%async_computation.4 | async-start | bytes 6684672 | tf_op jit(solution)/shard_map/all_gather | solution.py:16
  12.4 154.5 %reduce-scatter.5.cloned.1.call-start = ((), (), s32[]{:S(2)}) async-start(), calls=%async_computation.6 | async-start | bytes 4718592 | tf_op jit(solution)/shard_map/reduce_scatter | solution.py:98
  108.7 5.3 %copy-start = (bf16[2,512,2048]{2,1,0:T(8,128)(2,1)S(1)}, bf16[2,512,2048]{2,1,0:T(8,128)(2,1)}, u32[]{:S(2)}) copy-start(bf16[2,512,2048]{2,1,0:T(8,128)(2,1)} %all-gather.5.cloned.1.call-done) | copy-start | bytes 12582916
  108.7 5.9 %copy-start.2 = (bf16[2048,1536]{1,0:T(8,128)(2,1)S(1)}, bf16[2048,1536]{1,0:T(8,128)(2,1)}, u32[]{:S(2)}) copy-start(bf16[2048,1536]{1,0:T(8,128)(2,1)} %all-gather.3.cloned.1.call-done) | copy-start | bytes 18874372
  114.6 3.9 %copy-start.12 = (f32[1024,512]{1,0:T(8,128)}, f32[1024,512]{1,0:T(8,128)S(1)}, u32[]{:S(2)}) copy-start(f32[1024,512]{1,0:T(8,128)S(1)} %fusion.9) | copy-start | bytes 6291460
  129.2 0.7 copy-start.11
  129.2 41.9 %copy-start.3 = (bf16[64,2048]{1,0:T(8,128)(2,1)S(1)}, bf16[64,2048]{1,0:T(8,128)(2,1)}, u32[]{:S(2)}) copy-start(bf16[64,2048]{1,0:T(8,128)(2,1)} %param.13) | copy-start | bytes 786436
  129.3 174.6 %reduce-scatter.7.cloned.1.call-start = ((), (), s32[]{:S(2)}) async-start(), calls=%async_computation.7 | async-start | bytes 6684672
  201.6 1.6 copy-start.13
  201.6 2.2 copy-start.14
  203.8 3.3 %copy-start.1 = (bf16[2,512,2048]{2,1,0:T(8,128)(2,1)S(1)}, bf16[2,512,2048]{2,1,0:T(8,128)(2,1)}, u32[]{:S(2)}) copy-start(bf16[2,512,2048]{2,1,0:T(8,128)(2,1)} %all-gather.5.cloned.1.call-done) | copy-start | bytes 12582916
  229.4 3.8 %copy-start.7 = (f32[128,512]{1,0:T(8,128)S(1)}, f32[128,512]{1,0:T(8,128)}, u32[]{:S(2)}) copy-start(f32[128,512]{1,0:T(8,128)} %param.21) | copy-start | bytes 786436
  229.4 4.6 %copy-start.8 = (f32[128,512]{1,0:T(8,128)S(1)}, f32[128,512]{1,0:T(8,128)}, u32[]{:S(2)}) copy-start(f32[128,512]{1,0:T(8,128)} %param.20) | copy-start | bytes 786436
  229.4 5.5 %copy-start.9 = (f32[128,512]{1,0:T(8,128)S(1)}, f32[128,512]{1,0:T(8,128)}, u32[]{:S(2)}) copy-start(f32[128,512]{1,0:T(8,128)} %param.19) | copy-start | bytes 786436
  229.4 32.0 %copy-start.10 = (f32[2048]{0:T(1024)S(1)}, f32[2048]{0:T(1024)}, u32[]{:S(2)}) copy-start(f32[2048]{0:T(1024)} %param.14) | copy-start | bytes 24580
  229.4 30.9 %all-to-all-start.1 = ((bf16[8,64,2048]{2,1,0:T(8,128)(2,1)}), bf16[8,64,2048]{2,1,0:T(8,128)(2,1)S(1)}, u32[]{:S(2)}, u32[]{:S(2)}) async-start(bf16[8,64,2048]{2,1,0:T(8,128)(2,1)} %bitcast.14), calls=%async_computation.2 | async-start | bytes 4194304 | tf_op jit(solution)/shard_map/all_to_all | solution.py:45
  261.3 43.8 %copy-start.4 = (f32[128,512]{0,1:T(8,128)S(1)}, f32[128,512]{0,1:T(8,128)}, u32[]{:S(2)}) copy-start(f32[128,512]{0,1:T(8,128)} %copy.44) | copy-start | bytes 786436
  261.3 43.8 %copy-start.5 = (f32[128,512]{0,1:T(8,128)S(1)}, f32[128,512]{0,1:T(8,128)}, u32[]{:S(2)}) copy-start(f32[128,512]{0,1:T(8,128)} %copy.43) | copy-start | bytes 786436
  261.3 43.8 %copy-start.6 = (f32[128,512]{0,1:T(8,128)S(1)}, f32[128,512]{0,1:T(8,128)}, u32[]{:S(2)}) copy-start(f32[128,512]{0,1:T(8,128)} %copy.42) | copy-start | bytes 786436
Sparse Core Ops, SparseCore 0:
  10.6 34.4 all-gather.4
  47.3 61.3 all-gather.2
  129.4 37.4 reduce-scatter.4
  222.4 81.4 reduce-scatter.6
where the time goes:
time: 315 us; the launch traced here: 314 us
  waiting for transfers between devices  196 us (62%)
  blocking collectives  29.7 us (9%)
  matrix products  27.9 us (9%)
  local copies, waits for them, and re-layouts  27.4 us (9%)
  other arithmetic  15.7 us (5%)
  between operations  13.9 us (4%)
  starting transfers between devices  3.91 us (1%)
    all_gather x1, waiting for transfers between devices, sent_together(): lax.all_gather(both, axis, axis=dim, tiled=True)  63.5 us
    unnamed x5, waiting for transfers between devices  39.1 us
    reduce_scatter x1, waiting for transfers between devices, per_device(): lax.psum_scatter(gated_product.reshape(lax.axis_size('tp') * tok_rows, 2...  36.9 us
    all_gather x1, waiting for transfers between devices, per_device(): normed_rows = lax.all_gather(normed, 'tp', axis=1, tiled=True)  32.7 us
    all_to_all x1, blocking collectives, sent_to_all(): lax.all_to_all(jnp.broadcast_to(shard[None], (peers, *shard.shape)), axis...  29.7 us
    all_to_all x1, waiting for transfers between devices, summed_on_arrival(): lax.all_to_all(parts, axis, split_axis=0, concat_axis=0, tiled=True)  23.5 us
    unnamed x39, local copies, waits for them, and re-layouts  17.1 us
    dot_general x2, matrix products, contract_last(): lax.dot_general(first_op, second_op, (((1,), (1,)), ((), ())), preferred_...  7.09 us
  transfers between devices with their start and end apart: 5, of which 5 were waited for; matrix products, arithmetic and copies ran while one was open for 5% of the time, Pallas kernels for 0%

commit v1 on v0

--- a/solution.py
+++ b/solution.py
@@ -82,7 +82,13 @@
     input_rows = jnp.stack([late_input, early_input]).astype(jnp.float32)
     input_inverse = inverse_rms(input_rows)
     normed = (input_rows * input_inverse * pre_gain).astype(jnp.bfloat16)
-    normed_rows = lax.all_gather(normed, "tp", axis=1, tiled=True)
+    size = lax.axis_size("tp")
+    moving, blocks = (normed, [normed])
+    for _ in range(size - 1):
+        moving = lax.ppermute(moving, "tp", [(i, (i + 1) % size) for i in range(size)])
+        blocks.insert(0, moving)
+    line = jnp.concatenate(blocks, axis=1)
+    normed_rows = jnp.roll(line, (lax.axis_index("tp") + 1) * normed.shape[1], axis=1)
     gate_all, up_all, down_gradient_rows = sent_together(
         (gate_weight, up_weight, down_weight), "fs", 0, 1
     )

time: 315 us -> 302 us (0.959)
  blocking collectives: 29.7 us -> 0 us
  local copies, waits for them, and re-layouts: 27.4 us -> 39.3 us
  starting transfers between devices: 3.91 us -> 7.54 us
    ppermute x0 -> x7, waiting for transfers between devices: none -> 69.1 us  [per_device(): lax.ppermute(moving, 'tp', [(i, (i + 1) % size) for i in range(size)])]
    all_gather x1, waiting for transfers between devices: 63.5 us -> 0.01 us  [sent_together(): lax.all_gather(both, axis, axis=dim, tiled=True)]
    all_gather x1 -> x0, waiting for transfers between devices: 32.7 us -> none  [per_device(): normed_rows = lax.all_gather(normed, 'tp', axis=1, tiled=True)]
    all_to_all x1 -> x0, blocking collectives: 29.7 us -> none  [sent_to_all(): lax.all_to_all(jnp.broadcast_to(shard[None], (peers, *shard.shape)), axis...]
    all_to_all x0 -> x1, waiting for transfers between devices: none -> 26.9 us  [sent_to_all(): lax.all_to_all(jnp.broadcast_to(shard[None], (peers, *shard.shape)), axis...]
    unnamed x39 -> x53, local copies, waits for them, and re-layouts: 17.1 us -> 25.4 us
    all_to_all x0 -> x1, starting transfers between devices: none -> 3.6 us  [sent_to_all(): lax.all_to_all(jnp.broadcast_to(shard[None], (peers, *shard.shape)), axis...]
    unnamed x5 -> x4, waiting for transfers between devices: 39.1 us -> 40.7 us
  transfers between devices with their start and end apart: 5 -> 12, of which waited for: 5 -> 11; matrix products, arithmetic and copies ran while one was open for 5% -> 8% of each run, Pallas kernels for 0% -> 0%
where the time goes in v1:
time: 302 us; the launch traced here: 301 us
  waiting for transfers between devices  197 us (65%)
  local copies, waits for them, and re-layouts  39.3 us (13%)
  matrix products  28.1 us (9%)
  other arithmetic  14.7 us (5%)
  between operations  14.1 us (5%)
  starting transfers between devices  7.54 us (2%)
    ppermute x7, waiting for transfers between devices, per_device(): lax.ppermute(moving, 'tp', [(i, (i + 1) % size) for i in range(size)])  69.1 us
    unnamed x4, waiting for transfers between devices  40.7 us
    reduce_scatter x1, waiting for transfers between devices, per_device(): lax.psum_scatter(gated_product.reshape(lax.axis_size('tp') * tok_rows, 2...  38.1 us
    all_to_all x1, waiting for transfers between devices, sent_to_all(): lax.all_to_all(jnp.broadcast_to(shard[None], (peers, *shard.shape)), axis...  26.9 us
    unnamed x53, local copies, waits for them, and re-layouts  25.4 us
    all_to_all x1, waiting for transfers between devices, summed_on_arrival(): lax.all_to_all(parts, axis, split_axis=0, concat_axis=0, tiled=True)  22.6 us
    dot_general x2, matrix products, contract_last(): lax.dot_general(first_op, second_op, (((1,), (1,)), ((), ())), preferred_...  7.18 us
    convert_element_type x1, local copies, waits for them, and re-layouts, per_device(): gated_product.reshape(lax.axis_size('tp') * tok_rows, 2 * model_width)  6.4 us
  transfers between devices with their start and end apart: 12, of which 11 were waited for; matrix products, arithmetic and copies ran while one was open for 8% of the time, Pallas kernels for 0%

profile of v1, /device:TPU:0, one launch (start us, length us, event | category | flops | bytes accessed | tf_op | source)
XLA Modules:
  0.0 301.2 jit_solution(7106197401537910183)
XLA Ops:
  7.2 1.9 pad_maximum_fusion
  11.7 9.8 %collective-permute-done = bf16[2,64,2048]{2,1,0:T(8,128)(2,1)S(1)} collective-permute-done((bf16[2,64,2048]{2,1,0:T(8,128)(2,1)S(1)}, bf16[2,64,2048]{2,1,0:T(8,128)(2,1)S(1)}, u32[]{:S(2)}, u32[]{:S(2)}) %collective-permute-start) | collective-permute-done | bytes 524320 | tf_op jit(solution)/shard_map/ppermute | solution.py:88
  21.5 9.8 %collective-permute-done.1 = bf16[2,64,2048]{2,1,0:T(8,128)(2,1)S(1)} collective-permute-done((bf16[2,64,2048]{2,1,0:T(8,128)(2,1)S(1)}, bf16[2,64,2048]{2,1,0:T(8,128)(2,1)S(1)}, u32[]{:S(2)}, u32[]{:S(2)}) %collective-permute-start.1) | collective-permute-done | bytes 524320 | tf_op jit(solution)/shard_map/ppermute | solution.py:88
  31.3 9.8 %collective-permute-done.2 = bf16[2,64,2048]{2,1,0:T(8,128)(2,1)S(1)} collective-permute-done((bf16[2,64,2048]{2,1,0:T(8,128)(2,1)S(1)}, bf16[2,64,2048]{2,1,0:T(8,128)(2,1)S(1)}, u32[]{:S(2)}, u32[]{:S(2)}) %collective-permute-start.2) | collective-permute-done | bytes 524320 | tf_op jit(solution)/shard_map/ppermute | solution.py:88
  41.1 9.8 %collective-permute-done.3 = bf16[2,64,2048]{2,1,0:T(8,128)(2,1)S(1)} collective-permute-done((bf16[2,64,2048]{2,1,0:T(8,128)(2,1)S(1)}, bf16[2,64,2048]{2,1,0:T(8,128)(2,1)S(1)}, u32[]{:S(2)}, u32[]{:S(2)}) %collective-permute-start.3) | collective-permute-done | bytes 524320 | tf_op jit(solution)/shard_map/ppermute | solution.py:88
  50.9 9.8 %collective-permute-done.4 = bf16[2,64,2048]{2,1,0:T(8,128)(2,1)S(1)} collective-permute-done((bf16[2,64,2048]{2,1,0:T(8,128)(2,1)S(1)}, bf16[2,64,2048]{2,1,0:T(8,128)(2,1)S(1)}, u32[]{:S(2)}, u32[]{:S(2)}) %collective-permute-start.4) | collective-permute-done | bytes 524320 | tf_op jit(solution)/shard_map/ppermute | solution.py:88
  60.7 9.9 %collective-permute-done.5 = bf16[2,64,2048]{2,1,0:T(8,128)(2,1)} collective-permute-done((bf16[2,64,2048]{2,1,0:T(8,128)(2,1)S(1)}, bf16[2,64,2048]{2,1,0:T(8,128)(2,1)}, u32[]{:S(2)}, u32[]{:S(2)}) %collective-permute-start.5) | collective-permute-done | bytes 524320 | tf_op jit(solution)/shard_map/ppermute | solution.py:88
  70.7 10.1 %collective-permute-done.6 = bf16[2,64,2048]{2,1,0:T(8,128)(2,1)} collective-permute-done((bf16[2,64,2048]{2,1,0:T(8,128)(2,1)}, bf16[2,64,2048]{2,1,0:T(8,128)(2,1)}, u32[]{:S(2)}, u32[]{:S(2)}) %collective-permute-start.6) | collective-permute-done | bytes 524320 | tf_op jit(solution)/shard_map/ppermute | solution.py:88
  86.0 3.2 %copy-done = bf16[2,1024,2048]{2,1,0:T(8,128)(2,1)} copy-done((bf16[2,1024,2048]{2,1,0:T(8,128)(2,1)}, bf16[2,1024,2048]{2,1,0:T(8,128)(2,1)S(1)}, u32[]{:S(2)}) %copy-start) | copy-done | bytes 8388632
  89.2 2.3 constant_dynamic-slice_fusion
  91.5 5.3 %fusion.7 = f32[1024,512]{1,0:T(8,128)S(1)} fusion(bf16[1024,2048]{1,0:T(8,128)(2,1)} %bitcast.78, bf16[2048,1536]{1,0:T(8,128)(2,1)} %all-gather.2.cloned.1.call-done), kind=kOutput, calls=%fused_computation.12 | convolution fusion | flops 2147483648 | bytes 8388608 | tf_op jit(solution)/shard_map/dot_general | solution.py:96
  97.5 3.9 %multiply_convert_fusion = (bf16[1024,512]{1,0:T(8,128)(2,1)S(1)}, f32[1024,512]{1,0:T(8,128)}) fusion(f32[1024,512]{1,0:T(8,128)S(1)} %fusion.7, bf16[1024,2048]{1,0:T(8,128)(2,1)S(1)} %bitcast.79, bf16[2048,1536]{1,0:T(8,128)(2,1)S(1)} %copy-done.4), kind=kOutput, calls=%fused_computation.6 | convolution fusion | flops 2150629376 | bytes 11534336 | tf_op jit(solution)/shard_map/dot_general | solution.py:97
  101.4 4.4 %convolution_convert_fusion = bf16[2048,2,512]{2,0,1:T(8,128)(2,1)} fusion(bf16[2,512,512]{2,1,0:T(8,128)(2,1)S(1)} %bitcast.81, bf16[2048,1536]{1,0:T(8,128)(2,1)S(1)} %copy-done.4), kind=kOutput, calls=%fused_computation.3 | convolution fusion | flops 2149580800 | bytes 7340032 | tf_op jit(solution)/shard_map/utx,ix->tui/dot_general | solution.py:101
  105.8 6.4 %copy.39 = bf16[512,4096]{1,0:T(8,128)(2,1)} copy(bf16[512,4096]{0,1:T(8,128)(2,1)} %bitcast.80) | data formatting | bytes 8388608 | tf_op jit(solution)/shard_map/convert_element_type | solution.py:105
  112.3 38.1 %reduce-scatter.5.cloned.1.call-done = bf16[64,4096]{1,0:T(8,128)(2,1)} async-done(((bf16[512,4096]{1,0:T(8,128)(2,1)}), bf16[64,4096]{1,0:T(8,128)(2,1)}) %reduce-scatter.5.cloned.1.call-update) | async-done | bytes 524304 | tf_op jit(solution)/shard_map/reduce_scatter | solution.py:104
  150.4 2.1 reshape.128
  152.4 1.6 fusion.33
  155.2 1.6 broadcast_in_dim.2
  156.8 3.6 %all-to-all-start = ((bf16[8,64,2048]{2,1,0:T(8,128)(2,1)}), bf16[8,64,2048]{2,1,0:T(8,128)(2,1)S(1)}, u32[]{:S(2)}, u32[]{:S(2)}) async-start(bf16[8,64,2048]{2,1,0:T(8,128)(2,1)} %broadcast_in_dim.2), calls=%async_computation.1 | async-start | bytes 4194304 | tf_op jit(solution)/shard_map/all_to_all | solution.py:21
  160.6 26.9 %all-to-all-done = bf16[8,64,2048]{2,1,0:T(8,128)(2,1)S(1)} async-done(((bf16[8,64,2048]{2,1,0:T(8,128)(2,1)}), bf16[8,64,2048]{2,1,0:T(8,128)(2,1)S(1)}, u32[]{:S(2)}, u32[]{:S(2)}) %all-to-all-start) | async-done | bytes 2097184 | tf_op jit(solution)/shard_map/all_to_all | solution.py:21
  187.5 1.3 fusion.24
  189.7 3.4 %multiply_convert_fusion.1 = (bf16[512,512]{1,0:T(8,128)(2,1)S(1)}, bf16[512,512]{1,0:T(8,128)(2,1)S(1)}) fusion(f32[1024,512]{1,0:T(8,128)S(1)} %copy-done.11, f32[1024,512]{1,0:T(8,128)S(1)} %copy-done.12, bf16[512,2048]{1,0:T(8,128)(2,1)S(1)} %bitcast.65, bf16[2048,1536]{1,0:T(8,128)(2,1)} %all-gather.2.cloned.1.call-done), kind=kOutput, calls=%fused_computation.23 | convolution fusion | flops 1077149696 | bytes 7340032 | tf_op jit(solution)/shard_map/dot_general | solution.py:128
  193.1 1.3 fusion.12
  195.7 3.9 %fusion = bf16[2048,1536]{0,1:T(8,128)(2,1)} fusion(f32[2048,512]{0,1:T(8,128)S(1)} %fusion.24, f32[2048,512]{0,1:T(8,128)S(1)} %fusion.12, f32[2048,512]{0,1:T(8,128)S(1)} %fusion.13), kind=kLoop, calls=%fused_computation.1 | loop fusion | flops 12582912 | bytes 18874368 | tf_op jit(solution)/shard_map/convert_element_type | solution.py:163
  199.6 8.6 %copy.48 = bf16[2048,1536]{1,0:T(8,128)(2,1)} copy(bf16[2048,1536]{0,1:T(8,128)(2,1)} %fusion) | data formatting | bytes 12582912
  208.2 2.9 fusion.5
  211.1 4.3 %add_convert_fusion = bf16[512,2048]{1,0:T(8,128)(2,1)} fusion(f32[512,2048]{1,0:T(8,128)S(1)} %fusion.5, bf16[512,512]{1,0:T(8,128)(2,1)S(1)} %get-tuple-element.25, bf16[2048,1536]{1,0:T(8,128)(2,1)} %all-gather.2.cloned.1.call-done), kind=kOutput, calls=%fused_computation.2 | convolution fusion | flops 1075838976 | bytes 8912896 | tf_op jit(solution)/shard_map/dot_general | solution.py:50
  215.4 3.6 %all-to-all-start.1 = ((bf16[8,64,2048]{2,1,0:T(8,128)(2,1)}), bf16[8,64,2048]{2,1,0:T(8,128)(2,1)S(1)}, u32[]{:S(2)}, u32[]{:S(2)}) async-start(bf16[8,64,2048]{2,1,0:T(8,128)(2,1)} %bitcast.14), calls=%async_computation.2 | async-start | bytes 4194304 | tf_op jit(solution)/shard_map/all_to_all | solution.py:45
  220.7 1.8 copy.42
  223.6 22.6 %all-to-all-done.1 = bf16[8,64,2048]{2,1,0:T(8,128)(2,1)S(1)} async-done(((bf16[8,64,2048]{2,1,0:T(8,128)(2,1)}), bf16[8,64,2048]{2,1,0:T(8,128)(2,1)S(1)}, u32[]{:S(2)}, u32[]{:S(2)}) %all-to-all-start.1) | async-done | bytes 2097184 | tf_op jit(solution)/shard_map/all_to_all | solution.py:45
  246.7 2.2 fusion.23
  248.9 40.7 %reduce-scatter.7.cloned.1.call-done = bf16[128,1536]{1,0:T(8,128)(2,1)} async-done(((bf16[2048,1536]{1,0:T(8,128)(2,1)}), bf16[128,1536]{1,0:T(8,128)(2,1)}) %reduce-scatter.7.cloned.1.call-update) | async-done | bytes 393232
  (86 shorter events, 20.1 us)
Async XLA Ops:
  7.2 76.0 %copy-start.1 = (bf16[64,2048]{1,0:T(8,128)(2,1)S(1)}, bf16[64,2048]{1,0:T(8,128)(2,1)}, u32[]{:S(2)}) copy-start(bf16[64,2048]{1,0:T(8,128)(2,1)} %param.12) | copy-start | bytes 786436
  7.2 76.0 %copy-start.2 = (bf16[64,2048]{1,0:T(8,128)(2,1)S(1)}, bf16[64,2048]{1,0:T(8,128)(2,1)}, u32[]{:S(2)}) copy-start(bf16[64,2048]{1,0:T(8,128)(2,1)} %param.11) | copy-start | bytes 786436
  7.2 76.0 %copy-start.8 = (f32[2048]{0:T(1024)S(1)}, f32[2048]{0:T(1024)}, u32[]{:S(2)}) copy-start(f32[2048]{0:T(1024)} %param.14) | copy-start | bytes 24580
  7.2 84.3 %all-gather.2.cloned.1.call-start = ((), (), s32[]{:S(2)}) async-start(), calls=%async_computation.4 | async-start | bytes 6684672 | tf_op jit(solution)/shard_map/all_gather | solution.py:16
  9.1 141.2 %reduce-scatter.5.cloned.1.call-start = ((), (), s32[]{:S(2)}) async-start(), calls=%async_computation.5 | async-start | bytes 4718592 | tf_op jit(solution)/shard_map/reduce_scatter | solution.py:104
  11.6 9.8 %collective-permute-start = (bf16[2,64,2048]{2,1,0:T(8,128)(2,1)S(1)}, bf16[2,64,2048]{2,1,0:T(8,128)(2,1)S(1)}, u32[]{:S(2)}, u32[]{:S(2)}) collective-permute-start(bf16[2,64,2048]{2,1,0:T(8,128)(2,1)S(1)} %multiply_convert_fusion.2), channel_id=1, source_target_pairs={{0,1},{1,2},{2,3},{3,4},{4,5},{5,6},{6,7},{7,0},{8,9},{9,10},{10,1... | collective-permute-start | bytes 1572872 | tf_op jit(solution)/shard_map/ppermute | solution.py:88
  21.5 9.8 %collective-permute-start.1 = (bf16[2,64,2048]{2,1,0:T(8,128)(2,1)S(1)}, bf16[2,64,2048]{2,1,0:T(8,128)(2,1)S(1)}, u32[]{:S(2)}, u32[]{:S(2)}) collective-permute-start(bf16[2,64,2048]{2,1,0:T(8,128)(2,1)S(1)} %collective-permute-done), channel_id=1, source_target_pairs={{0,1},{1,2},{2,3},{3,4},{4,5},{5,6},{6,7},{7,0},{8,9},{9,10},{10,1... | collective-permute-start | bytes 1572872 | tf_op jit(solution)/shard_map/ppermute | solution.py:88
  31.3 9.8 %collective-permute-start.2 = (bf16[2,64,2048]{2,1,0:T(8,128)(2,1)S(1)}, bf16[2,64,2048]{2,1,0:T(8,128)(2,1)S(1)}, u32[]{:S(2)}, u32[]{:S(2)}) collective-permute-start(bf16[2,64,2048]{2,1,0:T(8,128)(2,1)S(1)} %collective-permute-done.1), channel_id=1, source_target_pairs={{0,1},{1,2},{2,3},{3,4},{4,5},{5,6},{6,7},{7,0},{8,9},{9,10},{10,1... | collective-permute-start | bytes 1572872 | tf_op jit(solution)/shard_map/ppermute | solution.py:88
  41.1 9.8 %collective-permute-start.3 = (bf16[2,64,2048]{2,1,0:T(8,128)(2,1)S(1)}, bf16[2,64,2048]{2,1,0:T(8,128)(2,1)S(1)}, u32[]{:S(2)}, u32[]{:S(2)}) collective-permute-start(bf16[2,64,2048]{2,1,0:T(8,128)(2,1)S(1)} %collective-permute-done.2), channel_id=1, source_target_pairs={{0,1},{1,2},{2,3},{3,4},{4,5},{5,6},{6,7},{7,0},{8,9},{9,10},{10,1... | collective-permute-start | bytes 1572872 | tf_op jit(solution)/shard_map/ppermute | solution.py:88
  50.9 9.8 %collective-permute-start.4 = (bf16[2,64,2048]{2,1,0:T(8,128)(2,1)S(1)}, bf16[2,64,2048]{2,1,0:T(8,128)(2,1)S(1)}, u32[]{:S(2)}, u32[]{:S(2)}) collective-permute-start(bf16[2,64,2048]{2,1,0:T(8,128)(2,1)S(1)} %collective-permute-done.3), channel_id=1, source_target_pairs={{0,1},{1,2},{2,3},{3,4},{4,5},{5,6},{6,7},{7,0},{8,9},{9,10},{10,1... | collective-permute-start | bytes 1572872 | tf_op jit(solution)/shard_map/ppermute | solution.py:88
  60.7 9.9 %collective-permute-start.5 = (bf16[2,64,2048]{2,1,0:T(8,128)(2,1)S(1)}, bf16[2,64,2048]{2,1,0:T(8,128)(2,1)}, u32[]{:S(2)}, u32[]{:S(2)}) collective-permute-start(bf16[2,64,2048]{2,1,0:T(8,128)(2,1)S(1)} %collective-permute-done.4), channel_id=1, source_target_pairs={{0,1},{1,2},{2,3},{3,4},{4,5},{5,6},{6,7},{7,0},{8,9},{9,10},{10,1... | collective-permute-start | bytes 1572872 | tf_op jit(solution)/shard_map/ppermute | solution.py:88
  70.7 10.1 %collective-permute-start.6 = (bf16[2,64,2048]{2,1,0:T(8,128)(2,1)}, bf16[2,64,2048]{2,1,0:T(8,128)(2,1)}, u32[]{:S(2)}, u32[]{:S(2)}) collective-permute-start(bf16[2,64,2048]{2,1,0:T(8,128)(2,1)} %collective-permute-done.5), channel_id=1, source_target_pairs={{0,1},{1,2},{2,3},{3,4},{4,5},{5,6},{6,7},{7,0},{8,9},{9,10},{10,1... | collective-permute-start | bytes 1572872 | tf_op jit(solution)/shard_map/ppermute | solution.py:88
  86.0 3.3 %copy-start = (bf16[2,1024,2048]{2,1,0:T(8,128)(2,1)}, bf16[2,1024,2048]{2,1,0:T(8,128)(2,1)S(1)}, u32[]{:S(2)}) copy-start(bf16[2,1024,2048]{2,1,0:T(8,128)(2,1)S(1)} %constant_dynamic-update-slice_fusion) | copy-start | bytes 25165828
  91.5 5.3 %copy-start.3 = (bf16[2,512,2048]{2,1,0:T(8,128)(2,1)S(1)}, bf16[2,512,2048]{2,1,0:T(8,128)(2,1)}, u32[]{:S(2)}) copy-start(bf16[2,512,2048]{2,1,0:T(8,128)(2,1)} %constant_dynamic-slice_fusion) | copy-start | bytes 12582916
  91.5 5.9 %copy-start.4 = (bf16[2048,1536]{1,0:T(8,128)(2,1)S(1)}, bf16[2048,1536]{1,0:T(8,128)(2,1)}, u32[]{:S(2)}) copy-start(bf16[2048,1536]{1,0:T(8,128)(2,1)} %all-gather.2.cloned.1.call-done) | copy-start | bytes 18874372
  97.5 3.9 %copy-start.10 = (f32[1024,512]{1,0:T(8,128)}, f32[1024,512]{1,0:T(8,128)S(1)}, u32[]{:S(2)}) copy-start(f32[1024,512]{1,0:T(8,128)S(1)} %fusion.7) | copy-start | bytes 6291460
  105.8 6.4 %copy-start.9 = (f32[2048]{0:T(1024)S(1)}, f32[2048]{0:T(1024)}, u32[]{:S(2)}) copy-start(f32[2048]{0:T(1024)} %param.15) | copy-start | bytes 24580
  112.2 42.4 %copy-start.5 = (bf16[64,2048]{1,0:T(8,128)(2,1)S(1)}, bf16[64,2048]{1,0:T(8,128)(2,1)}, u32[]{:S(2)}) copy-start(bf16[64,2048]{1,0:T(8,128)(2,1)} %param.13) | copy-start | bytes 786436
  156.8 30.7 %all-to-all-start = ((bf16[8,64,2048]{2,1,0:T(8,128)(2,1)}), bf16[8,64,2048]{2,1,0:T(8,128)(2,1)S(1)}, u32[]{:S(2)}, u32[]{:S(2)}) async-start(bf16[8,64,2048]{2,1,0:T(8,128)(2,1)} %broadcast_in_dim.2), calls=%async_computation.1 | async-start | bytes 4194304 | tf_op jit(solution)/shard_map/all_to_all | solution.py:21
  160.4 129.2 %reduce-scatter.7.cloned.1.call-start = ((), (), s32[]{:S(2)}) async-start(), calls=%async_computation.6 | async-start | bytes 6684672
  187.5 1.6 copy-start.11
  187.5 2.2 copy-start.12
  187.5 5.6 %slice-start = ((s8[8388608]{0:T(1024)(128)(4,1)}), s8[4194304]{0:T(1024)(128)(4,1)S(1)}, s32[]{:S(2)}) async-start(s8[8388608]{0:T(1024)(128)(4,1)} %bitcast.66), calls=%async_computation.7 | async-start | bytes 8388608
  189.7 3.4 %slice-start.1 = ((s8[8388608]{0:T(1024)(128)(4,1)}), s8[4194304]{0:T(1024)(128)(4,1)S(1)}, s32[]{:S(2)}) async-start(s8[8388608]{0:T(1024)(128)(4,1)} %bitcast.66), calls=%async_computation.8 | async-start | bytes 8388608
  211.1 7.9 %copy-start.6 = (f32[128,512]{1,0:T(8,128)S(1)}, f32[128,512]{1,0:T(8,128)}, u32[]{:S(2)}) copy-start(f32[128,512]{1,0:T(8,128)} %param.21) | copy-start | bytes 786436
  211.1 8.8 %copy-start.7 = (f32[128,512]{1,0:T(8,128)S(1)}, f32[128,512]{1,0:T(8,128)}, u32[]{:S(2)}) copy-start(f32[128,512]{1,0:T(8,128)} %param.20) | copy-start | bytes 786436
  215.4 30.7 %all-to-all-start.1 = ((bf16[8,64,2048]{2,1,0:T(8,128)(2,1)}), bf16[8,64,2048]{2,1,0:T(8,128)(2,1)S(1)}, u32[]{:S(2)}, u32[]{:S(2)}) async-start(bf16[8,64,2048]{2,1,0:T(8,128)(2,1)} %bitcast.14), calls=%async_computation.2 | async-start | bytes 4194304 | tf_op jit(solution)/shard_map/all_to_all | solution.py:45
Sparse Core Ops, SparseCore 0:
  10.1 63.8 all-gather.1
  112.4 37.9 reduce-scatter.4
  208.3 81.2 reduce-scatter.6
